TPU v7x, 32 devices: a whole 2x2x4 slice. The times are simulated.
32 devices in a mesh: sp: 4 (over z), tp: 8 (over y, x, core).
Axes of the slice: x: 2, y: 2, z: 4, core: 2. Of those that a mesh axis runs over, the one named last changes fastest.
Arguments:
- activations: bfloat16 [1024, 2048], P('sp', 'tp'), may hold values from -170 to 170
- norm_gain: float32 [2048], replicated, may hold values from 0.1 to 1.9
- query_weight: bfloat16 [2048, 1536], P(None, 'tp'), may hold values from -0.125 to 0.125
- latent_weight: bfloat16 [2048, 512], P(None, 'tp'), may hold values from -0.125 to 0.125
- rope_key_weight: bfloat16 [2048, 64], replicated, may hold values from -0.125 to 0.125
- latent_gain: float32 [512], replicated, may hold values from 1.5 to 64
- expand_weight: bfloat16 [512, 2048], P(None, 'tp'), may hold values from -0.25 to 0.25
- gate_weight: bfloat16 [2048, 1024], P(None, 'tp'), may hold values from -0.125 to 0.125
- pre_weight: bfloat16 [2048, 1024], P(None, 'tp'), may hold values from -0.125 to 0.125
- value_weight: bfloat16 [2048, 1024], P(None, 'tp'), may hold values from -0.125 to 0.125
- conv_kernel: bfloat16 [3, 1024], P(None, 'tp'), may hold values from -3.5 to 3.5
- output_attend: bfloat16 [1024, 2048], P('tp'), may hold values from -0.1875 to 0.1875
- output_conv: bfloat16 [1024, 2048], P('tp'), may hold values from -0.125 to 0.125
Outputs:
- mixed: bfloat16 [1024, 2048], P(('sp', 'tp'))
- log_weight_sum: float32 [8, 1024], P('tp', 'sp')
All inputs are finite; a program needn't handle non-finite values.
Results may differ from a plain program's by a relative error of at most 0.035.
The roundings to bfloat16 on the way count: a program that leaves them out, or rounds other values in their place, can miss the bound.
Values may be sent and summed in bfloat16 or wider, within the bound.
A program may use at most 128 MiB of HBM per device.

v0:
```python
import math
import jax
import jax.numpy as jnp
from jax import lax
from jax.sharding import PartitionSpec as P

D = 2048
NOPE = 128
ROPE = 64
VDIM = 128
GRID_W = 64
EPSILON = 1e-06
ROPE_BASE = 10000.0


def with_halo(array, sides, width):
    for axis, dim in sides:
        peers, length = (lax.axis_size(axis), array.shape[dim])
        up = [(i, (i + 1) % peers) for i in range(peers - 1)]
        down = [(j, i) for i, j in up]
        last = lax.slice_in_dim(array, length - width, length, axis=dim)
        leading = lax.slice_in_dim(array, 0, width, axis=dim)
        before = lax.ppermute(last, axis, up)
        after = lax.ppermute(leading, axis, down)
        array = jnp.concatenate([before, array, after], axis=dim)
    return array


def rotate(inputs, grid_rows, grid_cols):
    quarter = inputs.shape[-1] // 4
    inverse = ROPE_BASE ** (-jnp.arange(quarter, dtype=jnp.float32) / quarter)
    row_angle = (grid_rows[:, None] * inverse)[:, None, :]
    col_angle = (grid_cols[:, None] * inverse)[:, None, :]
    part_one = inputs[..., :quarter]
    part_two = inputs[..., quarter : 2 * quarter]
    part_three = inputs[..., 2 * quarter : 3 * quarter]
    part_four = inputs[..., 3 * quarter :]
    return jnp.concatenate(
        [
            part_one * jnp.cos(row_angle) - part_two * jnp.sin(row_angle),
            part_one * jnp.sin(row_angle) + part_two * jnp.cos(row_angle),
            part_three * jnp.cos(col_angle) - part_four * jnp.sin(col_angle),
            part_three * jnp.sin(col_angle) + part_four * jnp.cos(col_angle),
        ],
        axis=-1,
    )


def conv_branch(gate_proj, pre_proj, value_proj, conv_kernel):
    pre_mix = (pre_proj * value_proj).astype(jnp.bfloat16)
    padded = with_halo(pre_mix, (("sp", 0),), 1).astype(jnp.float32)
    kernel = conv_kernel.astype(jnp.float32)
    convolved = kernel[0] * padded[:-2] + kernel[1] * padded[1:-1] + kernel[2] * padded[2:]
    return (gate_proj * convolved).astype(jnp.bfloat16)


def body(
    activations,
    norm_gain,
    query_weight,
    latent_weight,
    rope_key_weight,
    latent_gain,
    expand_weight,
    gate_weight,
    pre_weight,
    value_weight,
    conv_kernel,
    output_attend,
    output_conv,
):
    tokens_here = activations.shape[0]
    query_cols = query_weight.shape[1]
    heads_here = query_cols // (NOPE + ROPE)
    latent_cols = latent_weight.shape[1]
    channels = gate_weight.shape[1]
    joined = jnp.concatenate(
        [query_weight, latent_weight, rope_key_weight, gate_weight, pre_weight, value_weight],
        axis=1,
    )
    inputs_f32 = activations.astype(jnp.float32)
    squares = lax.psum(jnp.sum(inputs_f32 * inputs_f32, axis=1, keepdims=True), "tp")
    partial_squares = jnp.zeros((tokens_here, 1), jnp.float32)
    piece_f32 = lax.all_gather(activations, "tp", axis=1, tiled=True).astype(jnp.float32)
    scaled = (piece_f32 * norm_gain).astype(jnp.bfloat16)
    running = jnp.dot(scaled, joined, preferred_element_type=jnp.float32)
    running, folded_squares = (running, partial_squares)
    inv_rms = lax.rsqrt(squares / D + EPSILON)
    projected = running * inv_rms
    latent_end = query_cols + latent_cols
    rope_end = latent_end + ROPE
    query_proj = projected[:, :query_cols]
    latent_proj = projected[:, query_cols:latent_end]
    rope_proj = projected[:, latent_end:rope_end]
    gate_proj = projected[:, rope_end : rope_end + channels]
    pre_proj = projected[:, rope_end + channels : rope_end + 2 * channels]
    value_proj = projected[:, rope_end + 2 * channels :]
    positions = lax.axis_index("sp") * tokens_here + jnp.arange(tokens_here, dtype=jnp.int32)
    grid_rows = (positions // GRID_W).astype(jnp.float32)
    grid_cols = (positions % GRID_W).astype(jnp.float32)
    query = query_proj.reshape(tokens_here, heads_here, NOPE + ROPE)
    query = jnp.concatenate(
        [query[..., :NOPE], rotate(query[..., NOPE:], grid_rows, grid_cols)], axis=-1
    )
    query = (query * (NOPE + ROPE) ** (-0.5)).astype(jnp.bfloat16)
    query_nope = query[..., :NOPE]
    query_rope = query[..., NOPE:]
    gathered = lax.all_gather(latent_proj.astype(jnp.bfloat16), "tp", axis=1, tiled=True).astype(
        jnp.float32
    )
    latent = (
        gathered
        * lax.rsqrt(jnp.mean(gathered * gathered, axis=1, keepdims=True) + EPSILON)
        * latent_gain
    ).astype(jnp.bfloat16)
    expanded = jnp.dot(latent, expand_weight, preferred_element_type=jnp.float32).astype(
        jnp.bfloat16
    )
    rope_key = rotate(rope_proj[:, None, :], grid_rows, grid_cols)[:, 0].astype(jnp.bfloat16)
    starting = (
        jnp.full((heads_here, tokens_here), -jnp.inf, jnp.float32),
        jnp.zeros((heads_here, tokens_here), jnp.float32),
        jnp.zeros((tokens_here, heads_here, VDIM), jnp.float32),
    )
    key_piece = lax.all_gather(expanded, "sp", axis=0, tiled=True)
    rope_piece = lax.all_gather(rope_key, "sp", axis=0, tiled=True)
    piece_rows = key_piece.shape[0]
    key_block = math.gcd(piece_rows, 1024)
    split_heads = key_piece.reshape(piece_rows, heads_here, NOPE + VDIM)

    def one_block(turn_index, state):
        row_max, row_sum, running_out = state
        offset = turn_index * key_block
        block_keys = lax.dynamic_slice_in_dim(split_heads, offset, key_block, 0)
        block_rope = lax.dynamic_slice_in_dim(rope_piece, offset, key_block, 0)
        scores = jnp.einsum(
            "thd,jhd->htj", query_nope, block_keys[..., :NOPE], preferred_element_type=jnp.float32
        )
        scores = scores + jnp.einsum(
            "thd,jd->htj", query_rope, block_rope, preferred_element_type=jnp.float32
        )
        new_max = jnp.maximum(row_max, jnp.max(scores, axis=-1))
        rescale = jnp.exp(row_max - new_max)
        weights = jnp.exp(scores - new_max[..., None])
        row_sum = row_sum * rescale + jnp.sum(weights, axis=-1)
        running_out = running_out * rescale.T[..., None] + jnp.einsum(
            "htj,jhd->thd",
            weights.astype(jnp.bfloat16),
            block_keys[..., NOPE:],
            preferred_element_type=jnp.float32,
        )
        return (new_max, row_sum, running_out)

    row_max, row_sum, running_out = lax.fori_loop(0, piece_rows // key_block, one_block, starting)
    attended = (
        (running_out / row_sum.T[..., None])
        .astype(jnp.bfloat16)
        .reshape(tokens_here, heads_here * VDIM)
    )
    log_weight_sum = row_max + jnp.log(row_sum)
    conv_mixed = conv_branch(gate_proj, pre_proj, value_proj, conv_kernel)
    mixed = lax.psum_scatter(
        (
            jnp.dot(attended, output_attend, preferred_element_type=jnp.float32)
            + jnp.dot(conv_mixed, output_conv, preferred_element_type=jnp.float32)
        ).astype(jnp.bfloat16),
        "tp",
        scatter_dimension=0,
        tiled=True,
    )
    return (mixed, log_weight_sum)


def solution(mesh):
    return jax.shard_map(
        body,
        mesh=mesh,
        in_specs=(
            P("sp", "tp"),
            P(),
            P(None, "tp"),
            P(None, "tp"),
            P(),
            P(),
            P(None, "tp"),
            P(None, "tp"),
            P(None, "tp"),
            P(None, "tp"),
            P(None, "tp"),
            P("tp", None),
            P("tp", None),
        ),
        out_specs=(P(("sp", "tp"), None), P("tp", "sp")),
        check_vma=False,
    )
```

profile of v0, /device:TPU:0, one launch (start us, length us, event | category | flops | bytes accessed | tf_op | source)
XLA Modules:
  0.0 135.6 jit_solution(17453811287171782455)
XLA Ops:
  7.2 0.0 copy-start
  7.2 0.0 copy-start.5
  7.2 0.0 copy-start.1
  7.2 0.0 copy-start.3
  7.2 0.0 copy-start.4
  7.2 0.0 all-gather.3.cloned.1.call-start
  7.3 0.7 all-gather.3.cloned.1.call-update
  8.0 0.0 reduce-scatter.2.cloned.1.call-start
  8.0 1.0 multiply_reduce_fusion
  9.0 1.2 copy.19
  10.3 1.3 copy.20
  11.5 1.2 copy.21
  12.8 15.2 %psum.7 = f32[256,1]{0,1:T(1,128)S(1)} all-reduce(f32[256,1]{0,1:T(1,128)S(1)} %bitcast.73), channel_id=1, replica_groups=mesh['sp'=4,'tp'=8] {'tp'}, use_global_device_ids=true, to_apply=%region_1.0 | all-reduce | flops 256 | bytes 2048 | tf_op jit(solution)/shard_map/psum | solution.py:82
  28.0 0.0 copy-done.5
  28.0 0.6 slice_bitcast_fusion.13
  28.6 0.0 copy-done.1
  28.6 0.9 constant_dynamic-update-slice_fusion.5
  29.5 0.0 copy-done.3
  29.6 0.7 constant_dynamic-update-slice_fusion.4
  30.3 0.7 constant_dynamic-update-slice_fusion.3
  31.0 0.8 constant_dynamic-update-slice_fusion.2
  31.8 0.9 constant_dynamic-update-slice_fusion.1
  32.7 0.8 constant_dynamic-update-slice_fusion
  33.5 2.7 %all-gather.3.cloned.1.call-done = bf16[256,2048]{1,0:T(8,128)(2,1)} async-done(((bf16[256,256]{1,0:T(8,128)(2,1)}), bf16[256,2048]{1,0:T(8,128)(2,1)}) %all-gather.3.cloned.1.call-update) | async-done | bytes 1048592 | tf_op jit(solution)/shard_map/all_gather | solution.py:84
  36.2 3.1 %convolution_multiply_fusion = f32[256,704]{0,1:T(8,128)S(1)} fusion(bf16[2048,704]{0,1:T(8,128)(2,1)} %constant_dynamic-update-slice_fusion, bf16[256,2048]{1,0:T(8,128)(2,1)} %all-gather.3.cloned.1.call-done, f32[2048]{0:T(1024)S(1)} %copy-done.7, f32[256]{0:T(256)S(1)} %bitcast.74), kind=kOutput, calls=%fused_computation.6 | convolution fusion | flops 739950592 | bytes 4662272 | tf_op jit(solution)/shard_map/dot_general | solution.py:86
  39.4 0.1 constant_dynamic-update-slice_fusion.9
  39.6 0.1 constant_dynamic-update-slice_fusion.8
  39.7 0.2 fusion.52
  39.9 13.4 %all-gather = bf16[1024,1,64]{0,2,1:T(8,128)(2,1)S(1)} all-gather(bf16[256,1,64]{0,2,1:T(8,128)(2,1)S(1)} %pad_maximum_fusion), channel_id=2, replica_groups=mesh['sp'=4,'tp'=8] {'sp'}, dimensions={0}, use_global_device_ids=true | all-gather | bytes 163840 | tf_op jit(solution)/shard_map/all_gather | solution.py:126
  53.4 0.1 constant_dynamic-update-slice_fusion.6
  53.5 9.3 %all_gather.13 = bf16[256,512]{0,1:T(8,128)(2,1)S(1)} all-gather(bf16[256,64]{0,1:T(8,128)(2,1)S(1)} %slice.196), channel_id=1, replica_groups=mesh['sp'=4,'tp'=8] {'tp'}, dimensions={1}, use_global_device_ids=true | all-gather | bytes 294912 | tf_op jit(solution)/shard_map/all_gather | solution.py:108
  62.8 0.1 fusion.10
  62.9 0.4 convolution_convert_fusion
  63.3 16.1 %all_gather.14 = bf16[1024,256]{1,0:T(8,128)(2,1)S(1)} all-gather(bf16[256,256]{1,0:T(8,128)(2,1)S(1)} %convolution_convert_fusion), channel_id=1, replica_groups=mesh['sp'=4,'tp'=8] {'sp'}, dimensions={0}, use_global_device_ids=true | all-gather | bytes 655360 | tf_op jit(solution)/shard_map/all_gather | solution.py:125
  79.4 0.3 convolution_bitcast_fusion.1
  79.7 0.4 fusion.66
  80.2 0.3 fusion.7
  80.5 0.1 fusion.65
  80.5 3.7 %collective-permute-start = (bf16[1,128]{0,1:T(8,128)(2,1)S(1)}, bf16[1,128]{0,1:T(8,128)(2,1)S(1)}, u32[]{:S(2)}, u32[]{:S(2)}) collective-permute-start(bf16[1,128]{0,1:T(8,128)(2,1)S(1)} %get-tuple-element.26), channel_id=1, source_target_pairs={{0,8},{8,16},{16,24},{1,9},{9,17},{17,25},{2,10},{10,18},{18,26},{... | collective-permute-start | bytes 776 | tf_op jit(solution)/shard_map/ppermute | solution.py:23
  84.2 1.3 collective-permute-start.1
  85.5 2.4 %fusion.9 = f32[256,2048]{1,0:T(8,128)} fusion(bf16[128,2048]{1,0:T(8,128)(2,1)S(1)} %copy-done, f32[1,256,1024]{2,1,0:T(8,128)S(1)} %get-tuple-element.44, f32[256]{0:T(256)S(1)} %get-tuple-element.43, bf16[1024,1,256]{2,0,1:T(8,128)(2,1)S(1)} %bitcast.70, f32[256]{0:T(256)S(1)} %get-tuple-element.42, f32[256]{0:T(256)S(1)} %get-tuple-element.41), kind=kOutput, calls=%fused_computation.19 | convolution fusion | flops 201949184 | bytes 3935232 | tf_op jit(solution)/shard_map/dot_general | solution.py:164
  88.0 0.0 collective-permute-done
  88.0 2.1 %collective-permute-done.1 = bf16[1,128]{0,1:T(8,128)(2,1)S(1)} collective-permute-done((bf16[1,128]{0,1:T(8,128)(2,1)S(1)}, bf16[1,128]{0,1:T(8,128)(2,1)S(1)}, u32[]{:S(2)}, u32[]{:S(2)}) %collective-permute-start.1) | collective-permute-done | bytes 288 | tf_op jit(solution)/shard_map/ppermute | solution.py:24
  90.0 0.1 maximum_convert_fusion
  90.2 3.2 %fusion = bf16[256,2048]{1,0:T(8,128)(2,1)} fusion(f32[256,2048]{1,0:T(8,128)} %fusion.9, bf16[128,2048]{1,0:T(8,128)(2,1)S(1)} %copy-done.2, f32[258,128]{0,1:T(8,128)S(1)} %maximum_convert_fusion, f32[256,704]{0,1:T(8,128)S(1)} %convolution_multiply_fusion, f32[128]{0:T(128)} %get-tuple-element.38, f32[128]{0:T(128)} %get-tuple-element.39, ...), kind=kOutput, calls=%fused_computation.1 | convolution fusion | flops 135495680 | bytes 4195840 | tf_op jit(solution)/shard_map/dot_general | solution.py:165
  93.4 0.0 reduce-scatter.2.cloned.1.call-update
  93.4 0.6 log_add_fusion
  94.0 34.8 %reduce-scatter.2.cloned.1.call-done = bf16[32,2048]{1,0:T(8,128)(2,1)} async-done(((bf16[256,2048]{1,0:T(8,128)(2,1)}), bf16[32,2048]{1,0:T(8,128)(2,1)}) %reduce-scatter.2.cloned.1.call-update) | async-done | bytes 131088 | tf_op jit(solution)/shard_map/reduce_scatter | solution.py:162
  (23 shorter events, 0.1 us)
Async XLA Ops:
  7.2 78.4 %copy-start = (bf16[128,2048]{1,0:T(8,128)(2,1)S(1)}, bf16[128,2048]{1,0:T(8,128)(2,1)}, u32[]{:S(2)}) copy-start(bf16[128,2048]{1,0:T(8,128)(2,1)} %param.24) | copy-start | bytes 1572868
  7.2 20.8 %copy-start.5 = (bf16[3,128]{1,0:T(4,128)(2,1)S(1)}, bf16[3,128]{1,0:T(4,128)(2,1)}, u32[]{:S(2)}) copy-start(bf16[3,128]{1,0:T(4,128)(2,1)} %param.23) | copy-start | bytes 2308
  7.2 21.4 %copy-start.1 = (bf16[2048,192]{0,1:T(8,128)(2,1)S(1)}, bf16[2048,192]{0,1:T(8,128)(2,1)}, u32[]{:S(2)}) copy-start(bf16[2048,192]{0,1:T(8,128)(2,1)} %param.15) | copy-start | bytes 2359300
  7.2 22.3 %copy-start.3 = (bf16[2048,64]{0,1:T(8,128)(2,1)S(1)}, bf16[2048,64]{0,1:T(8,128)(2,1)}, u32[]{:S(2)}) copy-start(bf16[2048,64]{0,1:T(8,128)(2,1)} %param.16) | copy-start | bytes 786436
  7.2 23.1 %copy-start.4 = (bf16[2048,64]{0,1:T(8,128)(2,1)S(1)}, bf16[2048,64]{0,1:T(8,128)(2,1)}, u32[]{:S(2)}) copy-start(bf16[2048,64]{0,1:T(8,128)(2,1)} %param.17) | copy-start | bytes 786436
  7.2 29.0 %all-gather.3.cloned.1.call-start = ((), (), s32[]{:S(2)}) async-start(), calls=%async_computation.1 | async-start | bytes 1179648 | tf_op jit(solution)/shard_map/all_gather | solution.py:84
  8.0 120.8 %reduce-scatter.2.cloned.1.call-start = ((), (), s32[]{:S(2)}) async-start(), calls=%async_computation.2 | async-start | bytes 1179648 | tf_op jit(solution)/shard_map/reduce_scatter | solution.py:162
  28.6 7.6 %copy-start.7 = (f32[2048]{0:T(1024)S(1)}, f32[2048]{0:T(1024)}, u32[]{:S(2)}) copy-start(f32[2048]{0:T(1024)} %param.14) | copy-start | bytes 24580
  36.2 26.7 %copy-start.6 = (bf16[512,256]{1,0:T(8,128)(2,1)S(1)}, bf16[512,256]{1,0:T(8,128)(2,1)}, u32[]{:S(2)}) copy-start(bf16[512,256]{1,0:T(8,128)(2,1)} %param.19) | copy-start | bytes 786436
  36.2 26.7 %copy-start.8 = (f32[512]{0:T(512)S(1)}, f32[512]{0:T(512)}, u32[]{:S(2)}) copy-start(f32[512]{0:T(512)} %param.18) | copy-start | bytes 6148
  80.1 10.0 %copy-start.2 = (bf16[128,2048]{1,0:T(8,128)(2,1)S(1)}, bf16[128,2048]{1,0:T(8,128)(2,1)}, u32[]{:S(2)}) copy-start(bf16[128,2048]{1,0:T(8,128)(2,1)} %param.25) | copy-start | bytes 1572868
  80.5 7.4 %collective-permute-start = (bf16[1,128]{0,1:T(8,128)(2,1)S(1)}, bf16[1,128]{0,1:T(8,128)(2,1)S(1)}, u32[]{:S(2)}, u32[]{:S(2)}) collective-permute-start(bf16[1,128]{0,1:T(8,128)(2,1)S(1)} %get-tuple-element.26), channel_id=1, source_target_pairs={{0,8},{8,16},{16,24},{1,9},{9,17},{17,25},{2,10},{10,18},{18,26},{... | collective-permute-start | bytes 776 | tf_op jit(solution)/shard_map/ppermute | solution.py:23
  84.2 5.8 %collective-permute-start.1 = (bf16[1,128]{0,1:T(8,128)(2,1)S(1)}, bf16[1,128]{0,1:T(8,128)(2,1)S(1)}, u32[]{:S(2)}, u32[]{:S(2)}) collective-permute-start(bf16[1,128]{0,1:T(8,128)(2,1)S(1)} %get-tuple-element.36), channel_id=1, source_target_pairs={{8,0},{16,8},{24,16},{9,1},{17,9},{25,17},{10,2},{18,10},{26,18},{... | collective-permute-start | bytes 776 | tf_op jit(solution)/shard_map/ppermute | solution.py:24
Sparse Core Ops, SparseCore 0:
  9.9 26.2 all-gather.2
  93.5 35.1 reduce-scatter.1
where the time goes:
time: 136 us
  blocking collectives  53.9 us (40%)
  waiting for transfers between devices  40.2 us (30%)
  between operations  14.3 us (11%)
  matrix products  9.9 us (7%)
  local copies, waits for them, and re-layouts  9.39 us (7%)
  starting transfers between devices  5.04 us (4%)
  other arithmetic  2.83 us (2%)
    reduce_scatter x1, waiting for transfers between devices, body(): lax.psum_scatter((jnp.dot(attended, output_attend, preferred_element_type...  34.8 us
    all_gather x1, blocking collectives, body(): key_piece = lax.all_gather(expanded, 'sp', axis=0, tiled=True)  16.1 us
    psum x1, blocking collectives, body(): lax.psum(jnp.sum(inputs_f32 * inputs_f32, axis=1, keepdims=True), 'tp')  15.2 us
    all_gather x1, blocking collectives, body(): rope_piece = lax.all_gather(rope_key, 'sp', axis=0, tiled=True)  13.4 us
    all_gather x1, blocking collectives, body(): lax.all_gather(latent_proj.astype(jnp.bfloat16), 'tp', axis=1, tiled=True)  9.26 us
    unnamed x27, local copies, waits for them, and re-layouts  7.86 us
    ppermute x1, starting transfers between devices, with_halo(): before = lax.ppermute(last, axis, up)  3.67 us
    dot_general x1, matrix products, body(): jnp.dot(conv_mixed, output_conv, preferred_element_type=jnp.float32)  3.22 us
  transfers between devices with their start and end apart: 4, of which 3 were waited for; matrix products, arithmetic and copies ran while one was open for 10% of the time, Pallas kernels for 0%

commit v1 on v0

--- a/solution.py
+++ b/solution.py
@@ -79,7 +79,9 @@
         axis=1,
     )
     inputs_f32 = activations.astype(jnp.float32)
-    squares = lax.psum(jnp.sum(inputs_f32 * inputs_f32, axis=1, keepdims=True), "tp")
+    squares = jnp.sum(
+        lax.all_gather(jnp.sum(inputs_f32 * inputs_f32, axis=1, keepdims=True), "tp"), 0
+    )
     partial_squares = jnp.zeros((tokens_here, 1), jnp.float32)
     piece_f32 = lax.all_gather(activations, "tp", axis=1, tiled=True).astype(jnp.float32)
     scaled = (piece_f32 * norm_gain).astype(jnp.bfloat16)

time: 136 us -> 136 us (level)
  blocking collectives: 53.9 us -> 49.2 us
  waiting for transfers between devices: 40.2 us -> 44.9 us
    psum x1 -> x0, blocking collectives: 15.2 us -> none  [body(): lax.psum(jnp.sum(inputs_f32 * inputs_f32, axis=1, keepdims=True), 'tp')]
    all_gather x0 -> x1, blocking collectives: none -> 10.4 us  [body(): lax.all_gather(jnp.sum(inputs_f32 * inputs_f32, axis=1, keepdims=True), '...]
    all_gather x1, waiting for transfers between devices: 2.68 us -> 7.34 us  [body(): lax.all_gather(activations, 'tp', axis=1, tiled=True).astype(jnp.float32)]
where the time goes in v1:
time: 136 us; the launch traced here: 135 us
  blocking collectives  49.2 us (36%)
  waiting for transfers between devices  44.9 us (33%)
  between operations  14.3 us (11%)
  matrix products  9.87 us (7%)
  local copies, waits for them, and re-layouts  9.39 us (7%)
  starting transfers between devices  5.05 us (4%)
  other arithmetic  2.86 us (2%)
    reduce_scatter x1, waiting for transfers between devices, body(): lax.psum_scatter((jnp.dot(attended, output_attend, preferred_element_type...  34.8 us
    all_gather x1, blocking collectives, body(): key_piece = lax.all_gather(expanded, 'sp', axis=0, tiled=True)  16.1 us
    all_gather x1, blocking collectives, body(): rope_piece = lax.all_gather(rope_key, 'sp', axis=0, tiled=True)  13.4 us
    all_gather x1, blocking collectives, body(): lax.all_gather(jnp.sum(inputs_f32 * inputs_f32, axis=1, keepdims=True), '...  10.4 us
    all_gather x1, blocking collectives, body(): lax.all_gather(latent_proj.astype(jnp.bfloat16), 'tp', axis=1, tiled=True)  9.25 us
    unnamed x27, local copies, waits for them, and re-layouts  7.86 us
    all_gather x1, waiting for transfers between devices, body(): lax.all_gather(activations, 'tp', axis=1, tiled=True).astype(jnp.float32)  7.34 us
    ppermute x1, starting transfers between devices, with_halo(): before = lax.ppermute(last, axis, up)  3.68 us
  transfers between devices with their start and end apart: 4, of which 3 were waited for; matrix products, arithmetic and copies ran while one was open for 10% of the time, Pallas kernels for 0%

profile of v1, /device:TPU:0, one launch (start us, length us, event | category | flops | bytes accessed | tf_op | source)
XLA Modules:
  0.0 135.5 jit_solution(6472867737686383588)
XLA Ops:
  7.2 0.0 copy-start
  7.2 0.0 copy-start.5
  7.2 0.0 copy-start.1
  7.2 0.0 copy-start.3
  7.2 0.0 copy-start.4
  7.2 0.0 all-gather.5.cloned.1.call-start
  7.3 0.7 all-gather.5.cloned.1.call-update
  8.0 0.0 reduce-scatter.2.cloned.1.call-start
  8.0 1.0 multiply_reduce_fusion
  9.0 1.2 copy.19
  10.3 1.3 copy.20
  11.5 1.2 copy.21
  12.8 10.4 %all-gather.2 = f32[8,1,256]{2,1,0:T(1,128)S(1)} all-gather(f32[1,1,256]{2,1,0:T(1,128)S(1)} %bitcast.72), channel_id=2, replica_groups=mesh['sp'=4,'tp'=8] {'tp'}, dimensions={0}, use_global_device_ids=true | all-gather | bytes 9216 | tf_op jit(solution)/shard_map/all_gather | solution.py:83
  23.2 0.0 copy-done.5
  23.3 0.6 slice_bitcast_fusion.13
  23.9 0.9 constant_dynamic-update-slice_fusion.5
  24.8 0.0 copy-done.3
  24.8 0.7 constant_dynamic-update-slice_fusion.4
  25.6 0.7 constant_dynamic-update-slice_fusion.3
  26.3 0.8 constant_dynamic-update-slice_fusion.2
  27.1 0.9 constant_dynamic-update-slice_fusion.1
  28.0 0.8 constant_dynamic-update-slice_fusion
  28.8 7.3 %all-gather.5.cloned.1.call-done = bf16[256,2048]{1,0:T(8,128)(2,1)} async-done(((bf16[256,256]{1,0:T(8,128)(2,1)}), bf16[256,2048]{1,0:T(8,128)(2,1)}) %all-gather.5.cloned.1.call-update) | async-done | bytes 1048592 | tf_op jit(solution)/shard_map/all_gather | solution.py:86
  36.1 0.0 copy-done.7
  36.1 3.1 %convolution_multiply_fusion = f32[256,704]{0,1:T(8,128)S(1)} fusion(bf16[2048,704]{0,1:T(8,128)(2,1)} %constant_dynamic-update-slice_fusion, bf16[256,2048]{1,0:T(8,128)(2,1)} %all-gather.5.cloned.1.call-done, f32[2048]{0:T(1024)S(1)} %copy-done.7, f32[256]{0:T(256)S(1)} %add_rsqrt_fusion.1), kind=kOutput, calls=%fused_computation.6 | convolution fusion | flops 739950592 | bytes 4662272 | tf_op jit(solution)/shard_map/dot_general | solution.py:88
  39.3 0.1 constant_dynamic-update-slice_fusion.9
  39.5 0.1 constant_dynamic-update-slice_fusion.8
  39.6 0.2 fusion.52
  39.9 13.4 %all-gather.1 = bf16[1024,1,64]{0,2,1:T(8,128)(2,1)S(1)} all-gather(bf16[256,1,64]{0,2,1:T(8,128)(2,1)S(1)} %pad_maximum_fusion), channel_id=3, replica_groups=mesh['sp'=4,'tp'=8] {'sp'}, dimensions={0}, use_global_device_ids=true | all-gather | bytes 163840 | tf_op jit(solution)/shard_map/all_gather | solution.py:128
  53.3 0.1 constant_dynamic-update-slice_fusion.6
  53.4 9.3 %all_gather.17 = bf16[256,512]{0,1:T(8,128)(2,1)S(1)} all-gather(bf16[256,64]{0,1:T(8,128)(2,1)S(1)} %slice.196), channel_id=1, replica_groups=mesh['sp'=4,'tp'=8] {'tp'}, dimensions={1}, use_global_device_ids=true | all-gather | bytes 294912 | tf_op jit(solution)/shard_map/all_gather | solution.py:110
  62.7 0.1 fusion.10
  62.8 0.4 convolution_convert_fusion
  63.2 16.1 %all_gather.18 = bf16[1024,256]{1,0:T(8,128)(2,1)S(1)} all-gather(bf16[256,256]{1,0:T(8,128)(2,1)S(1)} %convolution_convert_fusion), channel_id=1, replica_groups=mesh['sp'=4,'tp'=8] {'sp'}, dimensions={0}, use_global_device_ids=true | all-gather | bytes 655360 | tf_op jit(solution)/shard_map/all_gather | solution.py:127
  79.3 0.3 convolution_bitcast_fusion.1
  79.6 0.4 fusion.66
  80.1 0.3 fusion.7
  80.4 0.1 fusion.65
  80.5 3.7 %collective-permute-start = (bf16[1,128]{0,1:T(8,128)(2,1)S(1)}, bf16[1,128]{0,1:T(8,128)(2,1)S(1)}, u32[]{:S(2)}, u32[]{:S(2)}) collective-permute-start(bf16[1,128]{0,1:T(8,128)(2,1)S(1)} %get-tuple-element.26), channel_id=1, source_target_pairs={{0,8},{8,16},{16,24},{1,9},{9,17},{17,25},{2,10},{10,18},{18,26},{... | collective-permute-start | bytes 776 | tf_op jit(solution)/shard_map/ppermute | solution.py:23
  84.1 1.3 collective-permute-start.1
  85.5 2.4 %fusion.9 = f32[256,2048]{1,0:T(8,128)} fusion(bf16[128,2048]{1,0:T(8,128)(2,1)S(1)} %copy-done, f32[1,256,1024]{2,1,0:T(8,128)S(1)} %get-tuple-element.44, f32[256]{0:T(256)S(1)} %get-tuple-element.43, bf16[1024,1,256]{2,0,1:T(8,128)(2,1)S(1)} %bitcast.69, f32[256]{0:T(256)S(1)} %get-tuple-element.42, f32[256]{0:T(256)S(1)} %get-tuple-element.41), kind=kOutput, calls=%fused_computation.19 | convolution fusion | flops 201949184 | bytes 3935232 | tf_op jit(solution)/shard_map/dot_general | solution.py:166
  87.9 0.0 collective-permute-done
  87.9 2.1 %collective-permute-done.1 = bf16[1,128]{0,1:T(8,128)(2,1)S(1)} collective-permute-done((bf16[1,128]{0,1:T(8,128)(2,1)S(1)}, bf16[1,128]{0,1:T(8,128)(2,1)S(1)}, u32[]{:S(2)}, u32[]{:S(2)}) %collective-permute-start.1) | collective-permute-done | bytes 288 | tf_op jit(solution)/shard_map/ppermute | solution.py:24
  90.0 0.1 maximum_convert_fusion
  90.1 3.2 %fusion = bf16[256,2048]{1,0:T(8,128)(2,1)} fusion(f32[256,2048]{1,0:T(8,128)} %fusion.9, bf16[128,2048]{1,0:T(8,128)(2,1)S(1)} %copy-done.2, f32[258,128]{0,1:T(8,128)S(1)} %maximum_convert_fusion, f32[256,704]{0,1:T(8,128)S(1)} %convolution_multiply_fusion, f32[128]{0:T(128)} %get-tuple-element.38, f32[128]{0:T(128)} %get-tuple-element.39, ...), kind=kOutput, calls=%fused_computation.1 | convolution fusion | flops 135495680 | bytes 4195840 | tf_op jit(solution)/shard_map/dot_general | solution.py:167
  93.3 0.0 reduce-scatter.2.cloned.1.call-update
  93.3 0.6 log_add_fusion
  93.9 34.8 %reduce-scatter.2.cloned.1.call-done = bf16[32,2048]{1,0:T(8,128)(2,1)} async-done(((bf16[256,2048]{1,0:T(8,128)(2,1)}), bf16[32,2048]{1,0:T(8,128)(2,1)}) %reduce-scatter.2.cloned.1.call-update) | async-done | bytes 131088 | tf_op jit(solution)/shard_map/reduce_scatter | solution.py:164
  (24 shorter events, 0.2 us)
Async XLA Ops:
  7.2 78.3 %copy-start = (bf16[128,2048]{1,0:T(8,128)(2,1)S(1)}, bf16[128,2048]{1,0:T(8,128)(2,1)}, u32[]{:S(2)}) copy-start(bf16[128,2048]{1,0:T(8,128)(2,1)} %param.24) | copy-start | bytes 1572868
  7.2 16.1 %copy-start.5 = (bf16[3,128]{1,0:T(4,128)(2,1)S(1)}, bf16[3,128]{1,0:T(4,128)(2,1)}, u32[]{:S(2)}) copy-start(bf16[3,128]{1,0:T(4,128)(2,1)} %param.23) | copy-start | bytes 2308
  7.2 16.7 %copy-start.1 = (bf16[2048,192]{0,1:T(8,128)(2,1)S(1)}, bf16[2048,192]{0,1:T(8,128)(2,1)}, u32[]{:S(2)}) copy-start(bf16[2048,192]{0,1:T(8,128)(2,1)} %param.15) | copy-start | bytes 2359300
  7.2 17.6 %copy-start.3 = (bf16[2048,64]{0,1:T(8,128)(2,1)S(1)}, bf16[2048,64]{0,1:T(8,128)(2,1)}, u32[]{:S(2)}) copy-start(bf16[2048,64]{0,1:T(8,128)(2,1)} %param.16) | copy-start | bytes 786436
  7.2 18.4 %copy-start.4 = (bf16[2048,64]{0,1:T(8,128)(2,1)S(1)}, bf16[2048,64]{0,1:T(8,128)(2,1)}, u32[]{:S(2)}) copy-start(bf16[2048,64]{0,1:T(8,128)(2,1)} %param.17) | copy-start | bytes 786436
  7.2 28.9 %all-gather.5.cloned.1.call-start = ((), (), s32[]{:S(2)}) async-start(), calls=%async_computation.1 | async-start | bytes 1179648 | tf_op jit(solution)/shard_map/all_gather | solution.py:86
  8.0 120.7 %reduce-scatter.2.cloned.1.call-start = ((), (), s32[]{:S(2)}) async-start(), calls=%async_computation.2 | async-start | bytes 1179648 | tf_op jit(solution)/shard_map/reduce_scatter | solution.py:164
  23.9 12.3 %copy-start.7 = (f32[2048]{0:T(1024)S(1)}, f32[2048]{0:T(1024)}, u32[]{:S(2)}) copy-start(f32[2048]{0:T(1024)} %param.14) | copy-start | bytes 24580
  28.8 34.0 %copy-start.6 = (bf16[512,256]{1,0:T(8,128)(2,1)S(1)}, bf16[512,256]{1,0:T(8,128)(2,1)}, u32[]{:S(2)}) copy-start(bf16[512,256]{1,0:T(8,128)(2,1)} %param.19) | copy-start | bytes 786436
  28.8 34.0 %copy-start.8 = (f32[512]{0:T(512)S(1)}, f32[512]{0:T(512)}, u32[]{:S(2)}) copy-start(f32[512]{0:T(512)} %param.18) | copy-start | bytes 6148
  80.1 10.0 %copy-start.2 = (bf16[128,2048]{1,0:T(8,128)(2,1)S(1)}, bf16[128,2048]{1,0:T(8,128)(2,1)}, u32[]{:S(2)}) copy-start(bf16[128,2048]{1,0:T(8,128)(2,1)} %param.25) | copy-start | bytes 1572868
  80.5 7.4 %collective-permute-start = (bf16[1,128]{0,1:T(8,128)(2,1)S(1)}, bf16[1,128]{0,1:T(8,128)(2,1)S(1)}, u32[]{:S(2)}, u32[]{:S(2)}) collective-permute-start(bf16[1,128]{0,1:T(8,128)(2,1)S(1)} %get-tuple-element.26), channel_id=1, source_target_pairs={{0,8},{8,16},{16,24},{1,9},{9,17},{17,25},{2,10},{10,18},{18,26},{... | collective-permute-start | bytes 776 | tf_op jit(solution)/shard_map/ppermute | solution.py:23
  84.1 5.8 %collective-permute-start.1 = (bf16[1,128]{0,1:T(8,128)(2,1)S(1)}, bf16[1,128]{0,1:T(8,128)(2,1)S(1)}, u32[]{:S(2)}, u32[]{:S(2)}) collective-permute-start(bf16[1,128]{0,1:T(8,128)(2,1)S(1)} %get-tuple-element.36), channel_id=1, source_target_pairs={{8,0},{16,8},{24,16},{9,1},{17,9},{25,17},{10,2},{18,10},{26,18},{... | collective-permute-start | bytes 776 | tf_op jit(solution)/shard_map/ppermute | solution.py:24
Sparse Core Ops, SparseCore 0:
  9.9 26.1 all-gather.4
  93.4 35.1 reduce-scatter.1
